TPU v7x, 32 devices: a whole 2x2x4 slice. The times are simulated.
32 devices in a mesh: sp: 8 (over z, x), tp: 4 (over y, core).
Axes of the slice: x: 2, y: 2, z: 4, core: 2. Of those that a mesh axis runs over, the one named last changes fastest.
Arguments:
- tokens: bfloat16 [4096, 2048], P('sp', 'tp'), may hold values from -6 to 6
- norm_gain: float32 [2048], replicated, may hold values from 0.1 to 1.9
- w_query: bfloat16 [2048, 1024], P('sp', 'tp'), may hold values from -1 to 1
- w_key: bfloat16 [2048, 256], P('sp', 'tp'), may hold values from -16 to 16
- w_value: bfloat16 [2048, 256], P('sp', 'tp'), may hold values from -1 to 1
- w_post_gate: bfloat16 [2048, 1024], P('sp', 'tp'), may hold values from -0.125 to 0.125
- w_pre_gate: bfloat16 [2048, 1024], P('sp', 'tp'), may hold values from -0.125 to 0.125
- w_conv_in: bfloat16 [2048, 1024], P('sp', 'tp'), may hold values from -0.125 to 0.125
- conv_taps: float32 [3, 1024], P(None, 'tp'), may hold values from -3 to 3
- sink_logit: float32 [16], P('tp'), may hold values from 2 to 6
- w_out_attn: bfloat16 [1024, 2048], P('tp', 'sp'), may hold values from -0.1875 to 0.1875
- w_out_conv: bfloat16 [1024, 2048], P('tp', 'sp'), may hold values from -0.1875 to 0.1875
Outputs:
- mixed: bfloat16 [4096, 2048], P(('sp', 'tp'))
- log_weight_sum: float32 [16, 4096], P('tp', 'sp')
All inputs are finite; a program needn't handle non-finite values.
Results may differ from a plain program's by a relative error of at most 0.012.
The roundings to bfloat16 on the way count: a program that leaves them out, or rounds other values in their place, can miss the bound.
Values may be sent and summed in bfloat16 or wider, within the bound.
A program may use at most 64 MiB of HBM per device.

v0:
```python
import jax
import jax.numpy as jnp
from jax import lax
from jax.sharding import PartitionSpec as P

HEAD_DIM = 64
WINDOW = 128
GRID_W = 64
rope_base = 10000.0
norm_eps = 1e-06


def padded(block, sides, width):
    for axis, dim in sides:
        count = lax.axis_size(axis)
        forward = [(i, i + 1) for i in range(count - 1)]
        backward = [(target, source) for source, target in forward]
        low = lax.ppermute(
            lax.slice_in_dim(block, block.shape[dim] - width, None, axis=dim), axis, forward
        )
        high = lax.ppermute(lax.slice_in_dim(block, 0, width, axis=dim), axis, backward)
        block = jnp.concatenate([low, block, high], axis=dim)
    return block


def rotate_pair(values, angles):
    first_half, second_half = jnp.split(values, 2, axis=-1)
    cosine = jnp.cos(angles)[:, None, :]
    sine_part = jnp.sin(angles)[:, None, :]
    return jnp.concatenate(
        [
            first_half * cosine - second_half * sine_part,
            first_half * sine_part + second_half * cosine,
        ],
        axis=-1,
    )


def axial_rotate(values, positions):
    half_dim = values.shape[-1] // 2
    inv_freq = rope_base ** (-jnp.arange(0, half_dim, 2).astype(jnp.float32) / half_dim)
    row_angle = (positions // GRID_W).astype(jnp.float32)[:, None] * inv_freq
    col_angle = (positions % GRID_W).astype(jnp.float32)[:, None] * inv_freq
    row_part, col_part = jnp.split(values, 2, axis=-1)
    return jnp.concatenate(
        [rotate_pair(row_part, row_angle), rotate_pair(col_part, col_angle)], axis=-1
    )


def block_windows(source, rows_local, blocks):
    pieces = [
        source[step * WINDOW : step * WINDOW + rows_local].reshape(
            (blocks, WINDOW) + source.shape[1:]
        )
        for step in range(3)
    ]
    return jnp.concatenate(pieces, axis=1)


def on_device(
    tokens,
    norm_gain,
    w_query,
    w_key,
    w_value,
    w_post_gate,
    w_pre_gate,
    w_conv_in,
    conv_taps,
    sink_logit,
    w_out_attn,
    w_out_conv,
):
    whole = lax.all_gather(tokens, "tp", axis=1, tiled=True)
    rows_local = whole.shape[0]
    whole_float = whole.astype(jnp.float32)
    mean_square = jnp.mean(whole_float * whole_float, axis=1, keepdims=True)
    normed = (whole_float * lax.rsqrt(mean_square + norm_eps) * norm_gain).astype(jnp.bfloat16)
    col_widths = [
        w_query.shape[1],
        w_key.shape[1],
        w_value.shape[1],
        w_post_gate.shape[1],
        w_pre_gate.shape[1],
        w_conv_in.shape[1],
    ]
    joined = jnp.concatenate(
        (
            lax.all_gather(w_query, "sp", axis=0, tiled=True),
            lax.all_gather(w_key, "sp", axis=0, tiled=True),
            lax.all_gather(w_value, "sp", axis=0, tiled=True),
            lax.all_gather(w_post_gate, "sp", axis=0, tiled=True),
            lax.all_gather(w_pre_gate, "sp", axis=0, tiled=True),
            lax.all_gather(w_conv_in, "sp", axis=0, tiled=True),
        ),
        axis=1,
    )
    projected = jnp.dot(normed, joined, preferred_element_type=jnp.float32)
    bounds = []
    running = 0
    for col_width in col_widths[:-1]:
        running += col_width
        bounds.append(running)
    query_raw, key_raw, value_raw, post_gate, pre_gate, conv_input = jnp.split(
        projected, bounds, axis=1
    )
    offset = lax.axis_index("sp") * rows_local
    positions = offset + jnp.arange(rows_local, dtype=jnp.int32)
    local_heads = w_query.shape[1] // HEAD_DIM
    local_groups = w_key.shape[1] // HEAD_DIM
    group_size = local_heads // local_groups
    queries = axial_rotate(query_raw.reshape(rows_local, local_heads, HEAD_DIM), positions).astype(
        jnp.bfloat16
    )
    keys_rot = axial_rotate(key_raw.reshape(rows_local, local_groups, HEAD_DIM), positions).astype(
        jnp.bfloat16
    )
    key_value = jnp.concatenate(
        [keys_rot.reshape(rows_local, local_groups * HEAD_DIM), value_raw.astype(jnp.bfloat16)],
        axis=1,
    )
    mixed_input = (pre_gate * conv_input).astype(jnp.bfloat16)
    kv_padded = padded(key_value, (("sp", 0),), WINDOW)
    conv_padded = padded(mixed_input, (("sp", 0),), 1)
    conv_float = conv_padded.astype(jnp.float32)
    convolved = (
        conv_taps[0] * conv_float[:-2]
        + conv_taps[1] * conv_float[1:-1]
        + conv_taps[2] * conv_float[2:]
    )
    conv_out = (post_gate * convolved).astype(jnp.bfloat16)
    total_tokens = rows_local * lax.axis_size("sp")
    blocks = rows_local // WINDOW
    padded_rows = rows_local + 2 * WINDOW
    block_queries = queries.reshape(blocks, WINDOW, local_groups, group_size, HEAD_DIM)
    block_keys = block_windows(
        kv_padded[:, : local_groups * HEAD_DIM].reshape(padded_rows, local_groups, HEAD_DIM),
        rows_local,
        blocks,
    )
    block_values = block_windows(
        kv_padded[:, local_groups * HEAD_DIM :].reshape(padded_rows, local_groups, HEAD_DIM),
        rows_local,
        blocks,
    )
    scores = jnp.einsum(
        "nqkgd,nskd->nkgqs", block_queries, block_keys, preferred_element_type=jnp.float32
    ) * HEAD_DIM ** (-0.5)
    query_pos = positions.reshape(blocks, WINDOW)
    key_pos = (
        offset
        - WINDOW
        + (jnp.arange(blocks, dtype=jnp.int32) * WINDOW)[:, None]
        + jnp.arange(3 * WINDOW, dtype=jnp.int32)[None, :]
    )
    distance = key_pos[:, None, :] - query_pos[:, :, None]
    allowed = (
        (jnp.abs(distance) <= WINDOW)
        & (key_pos >= 0)[:, None, :]
        & (key_pos < total_tokens)[:, None, :]
    )
    scores = jnp.where(allowed[:, None, None], scores, -jnp.inf)
    sink_values = sink_logit.reshape(local_groups, group_size)[None, :, :, None]
    row_max = jnp.maximum(jnp.max(scores, axis=-1), sink_values)
    exp_scores = jnp.exp(scores - row_max[..., None])
    denominator = jnp.sum(exp_scores, axis=-1) + jnp.exp(sink_values - row_max)
    weights = (exp_scores / denominator[..., None]).astype(jnp.bfloat16)
    attended = (
        jnp.einsum("nkgqs,nskd->nqkgd", weights, block_values, preferred_element_type=jnp.float32)
        .astype(jnp.bfloat16)
        .reshape(rows_local, local_heads * HEAD_DIM)
    )
    log_sum = row_max + jnp.log(denominator)
    log_weight_sum = jnp.transpose(log_sum, (1, 2, 0, 3)).reshape(local_heads, rows_local)
    out_attn, out_conv = (
        lax.all_gather(w_out_attn, "sp", axis=1, tiled=True),
        lax.all_gather(w_out_conv, "sp", axis=1, tiled=True),
    )
    mixed = lax.psum_scatter(
        (
            jnp.dot(attended, out_attn, preferred_element_type=jnp.float32)
            + jnp.dot(conv_out, out_conv, preferred_element_type=jnp.float32)
        ).astype(jnp.bfloat16),
        "tp",
        scatter_dimension=0,
        tiled=True,
    )
    return (mixed, log_weight_sum)


def solution(mesh):
    placed = (
        P("sp", "tp"),
        P(),
        P("sp", "tp"),
        P("sp", "tp"),
        P("sp", "tp"),
        P("sp", "tp"),
        P("sp", "tp"),
        P("sp", "tp"),
        P(None, "tp"),
        P("tp"),
        P("tp", "sp"),
        P("tp", "sp"),
    )
    return jax.shard_map(
        on_device,
        mesh=mesh,
        in_specs=placed,
        out_specs=(P(("sp", "tp"), None), P("tp", "sp")),
        check_vma=False,
    )
```

profile of v0, /device:TPU:0, one launch (start us, length us, event | category | flops | bytes accessed | tf_op | source)
XLA Modules:
  0.0 326.0 jit_solution(14277394991578576114)
XLA Ops:
  7.2 0.7 all-gather.10.cloned.1.call-update
  7.9 0.0 all-gather.12.cloned.1.call-start
  7.9 0.7 all-gather.12.cloned.1.call-update
  8.6 0.0 all-gather.14.cloned.1.call-start
  8.7 0.7 all-gather.14.cloned.1.call-update
  9.4 0.5 all-gather.16.cloned.1.call-update
  10.0 0.5 all-gather.8.cloned.1.call-update
  10.6 0.5 all-gather.18.cloned.1.call-update
  11.2 0.7 all-gather.20.cloned.1.call-update
  11.9 0.0 reduce-scatter.2.cloned.1.call-start
  12.0 0.1 iota_add_fusion
  12.0 0.1 fusion.79
  12.1 0.9 copy.27
  13.0 34.2 %all_gather.29 = bf16[2048,64]{1,0:T(8,128)(2,1)S(1)} all-gather(bf16[256,64]{1,0:T(8,128)(2,1)S(1)} %copy.27), channel_id=1, replica_groups=mesh['sp'=8,'tp'=4] {'sp'}, dimensions={0}, use_global_device_ids=true | all-gather | bytes 294912 | tf_op jit(solution)/shard_map/all_gather | solution.py:90
  47.2 0.9 copy.28
  48.0 31.9 %all_gather.30 = bf16[2048,64]{1,0:T(8,128)(2,1)S(1)} all-gather(bf16[256,64]{1,0:T(8,128)(2,1)S(1)} %copy.28), channel_id=1, replica_groups=mesh['sp'=8,'tp'=4] {'sp'}, dimensions={0}, use_global_device_ids=true | all-gather | bytes 294912 | tf_op jit(solution)/shard_map/all_gather | solution.py:91
  79.9 1.4 fusion.91
  81.3 0.3 multiply_cosine_fusion.3
  81.6 0.9 fusion.18
  82.6 14.6 %all-gather.12.cloned.1.call-done = bf16[2048,256]{1,0:T(8,128)(2,1)} async-done(((bf16[256,256]{1,0:T(8,128)(2,1)}), bf16[2048,256]{1,0:T(8,128)(2,1)}) %all-gather.12.cloned.1.call-update) | async-done | bytes 1048592 | tf_op jit(solution)/shard_map/all_gather | solution.py:92
  97.2 41.2 %all-gather.14.cloned.1.call-done = bf16[2048,256]{1,0:T(8,128)(2,1)} async-done(((bf16[256,256]{1,0:T(8,128)(2,1)}), bf16[2048,256]{1,0:T(8,128)(2,1)}) %all-gather.14.cloned.1.call-update) | async-done | bytes 1048592 | tf_op jit(solution)/shard_map/all_gather | solution.py:93
  138.4 41.0 %all-gather.16.cloned.1.call-done = bf16[2048,256]{1,0:T(8,128)(2,1)} async-done(((bf16[256,256]{1,0:T(8,128)(2,1)}), bf16[2048,256]{1,0:T(8,128)(2,1)}) %all-gather.16.cloned.1.call-update) | async-done | bytes 1048592 | tf_op jit(solution)/shard_map/all_gather | solution.py:94
  179.4 8.2 %concatenate.68 = bf16[2048,1152]{1,0:T(8,128)(2,1)} concatenate(bf16[2048,256]{1,0:T(8,128)(2,1)} %all-gather.10.cloned.1.call-done, bf16[2048,64]{1,0:T(8,128)(2,1)S(1)} %all_gather.29, bf16[2048,64]{1,0:T(8,128)(2,1)S(1)} %all_gather.30, bf16[2048,256]{1,0:T(8,128)(2,1)} %all-gather.12.cloned.1.call-done, bf16[2048,256]{1,0:T(8,128)(2,1)} %all-gather.14.cloned.1.call-done, ...), dimensions={1} | concatenate | bytes 9437184 | tf_op jit(solution)/shard_map/concatenate | solution.py:87
  187.6 14.5 %all-gather.8.cloned.1.call-done = bf16[512,2048]{1,0:T(8,128)(2,1)} async-done(((bf16[512,512]{1,0:T(8,128)(2,1)}), bf16[512,2048]{1,0:T(8,128)(2,1)}) %all-gather.8.cloned.1.call-update) | async-done | bytes 2097168 | tf_op jit(solution)/shard_map/all_gather | solution.py:74
  202.1 2.1 fusion
  204.2 5.9 %fusion.5 = f32[512,1152]{1,0:T(8,128)S(1)} fusion(bf16[2048,1152]{1,0:T(8,128)(2,1)} %concatenate.68, bf16[512,2048]{1,0:T(8,128)(2,1)} %all-gather.8.cloned.1.call-done, f32[2048]{0:T(1024)S(1)} %copy-done.7, f32[512]{0:T(512)S(1)} %add_rsqrt_fusion), kind=kOutput, calls=%fused_computation.11 | convolution fusion | flops 2420113408 | bytes 9185280 | tf_op jit(solution)/shard_map/dot_general | solution.py:98
  210.1 0.1 fusion.23
  210.2 1.3 copy-done
  211.5 0.1 split.115
  211.6 0.2 copy.38
  211.8 0.1 fusion.71
  211.9 0.6 copy.62
  212.6 0.6 copy.63
  213.2 0.6 copy.64
  213.8 0.6 copy.65
  214.5 2.4 fusion.35
  216.8 0.3 concatenate.73
  217.1 3.4 %collective-permute-start = (bf16[128,128]{1,0:T(8,128)(2,1)S(1)}, bf16[128,128]{1,0:T(8,128)(2,1)S(1)}, u32[]{:S(2)}, u32[]{:S(2)}) collective-permute-start(bf16[128,128]{1,0:T(8,128)(2,1)S(1)} %get-tuple-element.24), channel_id=1, source_target_pairs={{0,4},{4,8},{8,12},{12,16},{16,20},{20,24},{24,28},{1,5},{5,9},{9,... | collective-permute-start | bytes 98312 | tf_op jit(solution)/shard_map/ppermute | solution.py:18
  220.5 1.3 collective-permute-start.1
  221.8 1.3 collective-permute-start.3
  223.1 5.2 %collective-permute-start.2 = (bf16[1,256]{1,0:T(2,128)(2,1)S(1)}, bf16[1,256]{1,0:T(2,128)(2,1)S(1)}, u32[]{:S(2)}, u32[]{:S(2)}) collective-permute-start(bf16[1,256]{1,0:T(2,128)(2,1)S(1)} %get-tuple-element.16), channel_id=1, source_target_pairs={{0,4},{4,8},{8,12},{12,16},{16,20},{20,24},{24,28},{1,5},{5,9},{9,... | collective-permute-start | bytes 1544 | tf_op jit(solution)/shard_map/ppermute | solution.py:18
  228.3 0.7 copy.35
  229.0 0.7 copy.34
  229.7 0.7 copy.33
  230.4 0.7 copy.32
  231.1 0.1 copy.30
  231.2 0.9 maximum_convert_fusion
  232.0 0.8 fusion.70
  232.8 0.7 copy.37
  233.6 0.7 copy.36
  234.3 1.7 fusion.4
  236.0 1.6 copy.31
  237.6 0.7 copy.29
  238.3 0.1 broadcast_maximum_fusion
  238.4 0.7 fusion.3
  239.1 0.1 exponential_add_fusion
  239.2 0.9 fusion.14
  240.2 0.2 copy.44
  240.4 3.1 all-gather.18.cloned.1.call-done
  243.4 4.1 %fusion.41 = f32[512,2048]{1,0:T(8,128)} fusion(bf16[256,2048]{1,0:T(8,128)(2,1)} %all-gather.18.cloned.1.call-done, bf16[32,8,4,128]{3,2,1,0:T(4,128)(2,1)S(1)} %bitcast.108), kind=kOutput, calls=%fused_computation.51 | convolution fusion | flops 536870912 | bytes 5505024 | tf_op jit(solution)/shard_map/dot_general | solution.py:181
  247.5 36.5 %all-gather.20.cloned.1.call-done = bf16[256,2048]{1,0:T(8,128)(2,1)} async-done(((bf16[256,256]{1,0:T(8,128)(2,1)}), bf16[256,2048]{1,0:T(8,128)(2,1)}) %all-gather.20.cloned.1.call-update) | async-done | bytes 1048592 | tf_op jit(solution)/shard_map/all_gather | solution.py:177
  284.0 4.8 %add_convert_fusion = bf16[512,2048]{1,0:T(8,128)(2,1)} fusion(f32[512,2048]{1,0:T(8,128)} %fusion.41, bf16[256,2048]{1,0:T(8,128)(2,1)} %all-gather.20.cloned.1.call-done, f32[514,256]{1,0:T(8,128)S(1)} %copy-done.1, f32[512,1152]{1,0:T(8,128)} %copy-done, f32[256]{0:T(256)S(1)} %bitcast.127, f32[256]{0:T(256)S(1)} %bitcast.128, f32[256]{0:T(256)S(1)} %bitcast.126), kind=kOutput, calls=%fused_computation.5 | convolution fusion | flops 539885568 | bytes 9440256 | tf_op jit(solution)/shard_map/dot_general | solution.py:182
  288.8 0.7 fusion.77
  289.5 29.6 %reduce-scatter.2.cloned.1.call-done = bf16[128,2048]{1,0:T(8,128)(2,1)} async-done(((bf16[512,2048]{1,0:T(8,128)(2,1)}), bf16[128,2048]{1,0:T(8,128)(2,1)}) %reduce-scatter.2.cloned.1.call-update) | async-done | bytes 524304 | tf_op jit(solution)/shard_map/reduce_scatter | solution.py:179
  (34 shorter events, 0.4 us)
Async XLA Ops:
  7.2 75.5 %all-gather.10.cloned.1.call-start = ((), (), s32[]{:S(2)}) async-start(), calls=%async_computation.2 | async-start | bytes 1179648 | tf_op jit(solution)/shard_map/all_gather | solution.py:89
  7.9 89.3 %all-gather.12.cloned.1.call-start = ((), (), s32[]{:S(2)}) async-start(), calls=%async_computation.3 | async-start | bytes 1179648 | tf_op jit(solution)/shard_map/all_gather | solution.py:92
  8.6 129.7 %all-gather.14.cloned.1.call-start = ((), (), s32[]{:S(2)}) async-start(), calls=%async_computation.4 | async-start | bytes 1179648 | tf_op jit(solution)/shard_map/all_gather | solution.py:93
  9.4 170.0 %all-gather.16.cloned.1.call-start = ((), (), s32[]{:S(2)}) async-start(), calls=%async_computation.5 | async-start | bytes 1179648 | tf_op jit(solution)/shard_map/all_gather | solution.py:94
  10.0 192.2 %all-gather.8.cloned.1.call-start = ((), (), s32[]{:S(2)}) async-start(), calls=%async_computation.1 | async-start | bytes 2621440 | tf_op jit(solution)/shard_map/all_gather | solution.py:74
  10.5 232.9 %all-gather.18.cloned.1.call-start = ((), (), s32[]{:S(2)}) async-start(), calls=%async_computation.6 | async-start | bytes 1179648 | tf_op jit(solution)/shard_map/all_gather | solution.py:176
  11.1 272.9 %all-gather.20.cloned.1.call-start = ((), (), s32[]{:S(2)}) async-start(), calls=%async_computation.7 | async-start | bytes 1179648 | tf_op jit(solution)/shard_map/all_gather | solution.py:177
  11.9 307.3 %reduce-scatter.2.cloned.1.call-start = ((), (), s32[]{:S(2)}) async-start(), calls=%async_computation.8 | async-start | bytes 2621440 | tf_op jit(solution)/shard_map/reduce_scatter | solution.py:179
  82.6 121.6 %copy-start.7 = (f32[2048]{0:T(1024)S(1)}, f32[2048]{0:T(1024)}, u32[]{:S(2)}) copy-start(f32[2048]{0:T(1024)} %param.13) | copy-start | bytes 24580
  210.1 1.4 copy-start
  217.1 14.9 %collective-permute-start = (bf16[128,128]{1,0:T(8,128)(2,1)S(1)}, bf16[128,128]{1,0:T(8,128)(2,1)S(1)}, u32[]{:S(2)}, u32[]{:S(2)}) collective-permute-start(bf16[128,128]{1,0:T(8,128)(2,1)S(1)} %get-tuple-element.24), channel_id=1, source_target_pairs={{0,4},{4,8},{8,12},{12,16},{16,20},{20,24},{24,28},{1,5},{5,9},{9,... | collective-permute-start | bytes 98312 | tf_op jit(solution)/shard_map/ppermute | solution.py:18
  220.5 11.5 %collective-permute-start.1 = (bf16[128,128]{1,0:T(8,128)(2,1)S(1)}, bf16[128,128]{1,0:T(8,128)(2,1)S(1)}, u32[]{:S(2)}, u32[]{:S(2)}) collective-permute-start(bf16[128,128]{1,0:T(8,128)(2,1)S(1)} %get-tuple-element.25), channel_id=1, source_target_pairs={{4,0},{8,4},{12,8},{16,12},{20,16},{24,20},{28,24},{5,1},{9,5},{13... | collective-permute-start | bytes 98312 | tf_op jit(solution)/shard_map/ppermute | solution.py:21
  221.8 9.3 %collective-permute-start.3 = (bf16[1,256]{1,0:T(2,128)(2,1)S(1)}, bf16[1,256]{1,0:T(2,128)(2,1)S(1)}, u32[]{:S(2)}, u32[]{:S(2)}) collective-permute-start(bf16[1,256]{1,0:T(2,128)(2,1)S(1)} %get-tuple-element.17), channel_id=1, source_target_pairs={{4,0},{8,4},{12,8},{16,12},{20,16},{24,20},{28,24},{5,1},{9,5},{13... | collective-permute-start | bytes 1544 | tf_op jit(solution)/shard_map/ppermute | solution.py:21
  223.1 8.0 %collective-permute-start.2 = (bf16[1,256]{1,0:T(2,128)(2,1)S(1)}, bf16[1,256]{1,0:T(2,128)(2,1)S(1)}, u32[]{:S(2)}, u32[]{:S(2)}) collective-permute-start(bf16[1,256]{1,0:T(2,128)(2,1)S(1)} %get-tuple-element.16), channel_id=1, source_target_pairs={{0,4},{4,8},{8,12},{12,16},{16,20},{20,24},{24,28},{1,5},{5,9},{9,... | collective-permute-start | bytes 1544 | tf_op jit(solution)/shard_map/ppermute | solution.py:18
  232.8 5.5 %copy-start.4 = (f32[4]{0:T(128)S(1)}, f32[4]{0:T(128)}, u32[]{:S(2)}) copy-start(f32[4]{0:T(128)} %param.21) | copy-start | bytes 52
  238.3 0.8 copy-start.2
  238.3 0.9 copy-start.3
  243.4 40.6 %copy-start.1 = (f32[514,256]{1,0:T(8,128)S(1)}, f32[514,256]{1,0:T(8,128)}, u32[]{:S(2)}) copy-start(f32[514,256]{1,0:T(8,128)} %maximum_convert_fusion) | copy-start | bytes 1579012
  243.4 40.6 %copy-start.5 = (f32[1,256]{1,0:T(1,128)S(1)}, f32[1,256]{1,0:T(1,128)}, u32[]{:S(2)}) copy-start(f32[1,256]{1,0:T(1,128)} %get-tuple-element.27) | copy-start | bytes 3076
  243.4 40.6 %copy-start.6 = (f32[1,256]{1,0:T(1,128)S(1)}, f32[1,256]{1,0:T(1,128)}, u32[]{:S(2)}) copy-start(f32[1,256]{1,0:T(1,128)} %get-tuple-element.28) | copy-start | bytes 3076
Sparse Core Ops, SparseCore 0:
  10.1 45.7 all-gather.9
  58.0 39.1 all-gather.11
  99.4 38.9 all-gather.13
  140.4 38.9 all-gather.15
  180.8 21.2 all-gather.7
  204.0 39.3 all-gather.17
  245.5 38.4 all-gather.19
  288.9 30.1 reduce-scatter.1
where the time goes:
time: 327 us; the launch traced here: 326 us
  waiting for transfers between devices  185 us (57%)
  blocking collectives  66.1 us (20%)
  local copies, waits for them, and re-layouts  22.7 us (7%)
  matrix products  17.4 us (5%)
  between operations  14.4 us (4%)
  starting transfers between devices  11.4 us (3%)
  other arithmetic  9.22 us (3%)
    all_gather x1, waiting for transfers between devices, on_device(): lax.all_gather(w_pre_gate, 'sp', axis=0, tiled=True)  41.2 us
    all_gather x1, waiting for transfers between devices, on_device(): lax.all_gather(w_conv_in, 'sp', axis=0, tiled=True)  41 us
    all_gather x1, waiting for transfers between devices, on_device(): lax.all_gather(w_out_conv, 'sp', axis=1, tiled=True)  36.5 us
    all_gather x1, blocking collectives, on_device(): lax.all_gather(w_key, 'sp', axis=0, tiled=True)  34.2 us
    all_gather x1, blocking collectives, on_device(): lax.all_gather(w_value, 'sp', axis=0, tiled=True)  31.9 us
    reduce_scatter x1, waiting for transfers between devices, on_device(): lax.psum_scatter((jnp.dot(attended, out_attn, preferred_element_type=jnp....  29.6 us
    all_gather x1, waiting for transfers between devices, on_device(): lax.all_gather(w_post_gate, 'sp', axis=0, tiled=True)  14.6 us
    all_gather x1, waiting for transfers between devices, on_device(): whole = lax.all_gather(tokens, 'tp', axis=1, tiled=True)  14.5 us
  transfers between devices with their start and end apart: 12, of which 7 were waited for; matrix products, arithmetic and copies ran while one was open for 13% of the time, Pallas kernels for 0%

commit v1 on v0

--- a/solution.py
+++ b/solution.py
@@ -174,7 +174,7 @@
     log_weight_sum = jnp.transpose(log_sum, (1, 2, 0, 3)).reshape(local_heads, rows_local)
     out_attn, out_conv = (
         lax.all_gather(w_out_attn, "sp", axis=1, tiled=True),
-        lax.all_gather(w_out_conv, "sp", axis=1, tiled=True),
+        jnp.concatenate(lax.all_gather(w_out_conv, "sp"), axis=1),
     )
     mixed = lax.psum_scatter(
         (

time: 327 us -> 328 us (level)
  waiting for transfers between devices: 185 us -> 199 us
  local copies, waits for them, and re-layouts: 22.7 us -> 15.4 us
  matrix products: 17.4 us -> 12.6 us
    all_gather x1, waiting for transfers between devices: 36.5 us -> 0.02 us  [on_device(): lax.all_gather(w_out_conv, 'sp')]
    all_gather x1, waiting for transfers between devices: 14.6 us -> 41.1 us  [on_device(): lax.all_gather(w_post_gate, 'sp', axis=0, tiled=True)]
    all_gather x1, waiting for transfers between devices: 0.02 us -> 13.8 us  [on_device(): lax.all_gather(w_query, 'sp', axis=0, tiled=True)]
    all_gather x1, waiting for transfers between devices: 3.06 us -> 13.1 us  [on_device(): lax.all_gather(w_out_attn, 'sp', axis=1, tiled=True)]
    concatenate x8, local copies, waits for them, and re-layouts: 5.27 us -> 0.41 us  [axial_rotate(): jnp.concatenate([rotate_pair(row_part, row_angle), rotate_pair(col_part,...]
    reshape x5, local copies, waits for them, and re-layouts: 3.89 us -> 0.56 us  [block_windows(): source[step * WINDOW:step * WINDOW + rows_local]]
  transfers between devices with their start and end apart: 12 -> 12, of which waited for: 7 -> 8; matrix products, arithmetic and copies ran while one was open for 13% -> 9% of each run, Pallas kernels for 0% -> 0%
where the time goes in v1:
time: 328 us; the launch traced here: 327 us
  waiting for transfers between devices  199 us (61%)
  blocking collectives  66.1 us (20%)
  local copies, waits for them, and re-layouts  15.4 us (5%)
  between operations  14.4 us (4%)
  matrix products  12.6 us (4%)
  starting transfers between devices  11.4 us (3%)
  other arithmetic  7.79 us (2%)
    all_gather x1, waiting for transfers between devices, on_device(): lax.all_gather(w_post_gate, 'sp', axis=0, tiled=True)  41.1 us
    all_gather x1, waiting for transfers between devices, on_device(): lax.all_gather(w_pre_gate, 'sp', axis=0, tiled=True)  41 us
    all_gather x1, waiting for transfers between devices, on_device(): lax.all_gather(w_conv_in, 'sp', axis=0, tiled=True)  41 us
    all_gather x1, blocking collectives, on_device(): lax.all_gather(w_key, 'sp', axis=0, tiled=True)  34.2 us
    all_gather x1, blocking collectives, on_device(): lax.all_gather(w_value, 'sp', axis=0, tiled=True)  31.9 us
    reduce_scatter x1, waiting for transfers between devices, on_device(): lax.psum_scatter((jnp.dot(attended, out_attn, preferred_element_type=jnp....  29.6 us
    all_gather x1, waiting for transfers between devices, on_device(): whole = lax.all_gather(tokens, 'tp', axis=1, tiled=True)  14.5 us
    all_gather x1, waiting for transfers between devices, on_device(): lax.all_gather(w_query, 'sp', axis=0, tiled=True)  13.8 us
  transfers between devices with their start and end apart: 12, of which 8 were waited for; matrix products, arithmetic and copies ran while one was open for 9% of the time, Pallas kernels for 0%

profile of v1, /device:TPU:0, one launch (start us, length us, event | category | flops | bytes accessed | tf_op | source)
XLA Modules:
  0.0 326.9 jit_solution(6766843247825071561)
XLA Ops:
  7.2 0.7 all-gather.21.cloned.1.call-update
  7.9 0.0 all-gather.11.cloned.1.call-start
  7.9 0.7 all-gather.11.cloned.1.call-update
  8.7 0.7 all-gather.13.cloned.1.call-update
  9.4 0.0 all-gather.15.cloned.1.call-start
  9.4 0.5 all-gather.15.cloned.1.call-update
  10.0 0.0 all-gather.17.cloned.1.call-start
  10.0 0.5 all-gather.17.cloned.1.call-update
  10.6 0.5 all-gather.9.cloned.1.call-update
  11.1 0.0 all-gather.19.cloned.1.call-start
  11.2 0.7 all-gather.19.cloned.1.call-update
  11.9 0.0 reduce-scatter.2.cloned.1.call-start
  11.9 0.1 iota_add_fusion
  12.0 0.1 fusion.79
  12.1 0.9 copy.46
  13.0 34.2 %all_gather.32 = bf16[2048,64]{1,0:T(8,128)(2,1)S(1)} all-gather(bf16[256,64]{1,0:T(8,128)(2,1)S(1)} %copy.46), channel_id=1, replica_groups=mesh['sp'=8,'tp'=4] {'sp'}, dimensions={0}, use_global_device_ids=true | all-gather | bytes 294912 | tf_op jit(solution)/shard_map/all_gather | solution.py:90
  47.2 0.9 copy.47
  48.0 31.9 %all_gather.33 = bf16[2048,64]{1,0:T(8,128)(2,1)S(1)} all-gather(bf16[256,64]{1,0:T(8,128)(2,1)S(1)} %copy.47), channel_id=1, replica_groups=mesh['sp'=8,'tp'=4] {'sp'}, dimensions={0}, use_global_device_ids=true | all-gather | bytes 294912 | tf_op jit(solution)/shard_map/all_gather | solution.py:91
  79.9 0.8 fusion.91
  80.7 0.3 multiply_cosine_fusion.3
  81.1 0.9 fusion.18
  82.0 1.5 copy.64
  83.5 13.8 %all-gather.11.cloned.1.call-done = bf16[2048,256]{1,0:T(8,128)(2,1)} async-done(((bf16[256,256]{1,0:T(8,128)(2,1)}), bf16[2048,256]{1,0:T(8,128)(2,1)}) %all-gather.11.cloned.1.call-update) | async-done | bytes 1048592 | tf_op jit(solution)/shard_map/all_gather | solution.py:89
  97.3 41.1 %all-gather.13.cloned.1.call-done = bf16[2048,256]{1,0:T(8,128)(2,1)} async-done(((bf16[256,256]{1,0:T(8,128)(2,1)}), bf16[2048,256]{1,0:T(8,128)(2,1)}) %all-gather.13.cloned.1.call-update) | async-done | bytes 1048592 | tf_op jit(solution)/shard_map/all_gather | solution.py:92
  138.4 41.0 %all-gather.15.cloned.1.call-done = bf16[2048,256]{1,0:T(8,128)(2,1)} async-done(((bf16[256,256]{1,0:T(8,128)(2,1)}), bf16[2048,256]{1,0:T(8,128)(2,1)}) %all-gather.15.cloned.1.call-update) | async-done | bytes 1048592 | tf_op jit(solution)/shard_map/all_gather | solution.py:93
  179.4 41.0 %all-gather.17.cloned.1.call-done = bf16[2048,256]{1,0:T(8,128)(2,1)} async-done(((bf16[256,256]{1,0:T(8,128)(2,1)}), bf16[2048,256]{1,0:T(8,128)(2,1)}) %all-gather.17.cloned.1.call-update) | async-done | bytes 1048592 | tf_op jit(solution)/shard_map/all_gather | solution.py:94
  220.4 8.2 %concatenate.68 = bf16[2048,1152]{1,0:T(8,128)(2,1)} concatenate(bf16[2048,256]{1,0:T(8,128)(2,1)} %all-gather.11.cloned.1.call-done, bf16[2048,64]{1,0:T(8,128)(2,1)S(1)} %all_gather.32, bf16[2048,64]{1,0:T(8,128)(2,1)S(1)} %all_gather.33, bf16[2048,256]{1,0:T(8,128)(2,1)} %all-gather.13.cloned.1.call-done, bf16[2048,256]{1,0:T(8,128)(2,1)} %all-gather.15.cloned.1.call-done, ...), dimensions={1} | concatenate | bytes 9437184 | tf_op jit(solution)/shard_map/concatenate | solution.py:87
  228.7 14.5 %all-gather.9.cloned.1.call-done = bf16[512,2048]{1,0:T(8,128)(2,1)} async-done(((bf16[512,512]{1,0:T(8,128)(2,1)}), bf16[512,2048]{1,0:T(8,128)(2,1)}) %all-gather.9.cloned.1.call-update) | async-done | bytes 2097168 | tf_op jit(solution)/shard_map/all_gather | solution.py:74
  243.2 2.1 fusion
  245.2 5.9 %fusion.5 = f32[512,1152]{1,0:T(8,128)S(1)} fusion(bf16[2048,1152]{1,0:T(8,128)(2,1)} %concatenate.68, bf16[512,2048]{1,0:T(8,128)(2,1)} %all-gather.9.cloned.1.call-done, f32[2048]{0:T(1024)S(1)} %copy-done.2, f32[512]{0:T(512)S(1)} %add_rsqrt_fusion), kind=kOutput, calls=%fused_computation.11 | convolution fusion | flops 2420113408 | bytes 9185280 | tf_op jit(solution)/shard_map/dot_general | solution.py:98
  251.2 0.1 fusion.23
  251.3 1.3 copy-done
  252.6 0.1 split.115
  252.7 0.2 copy.57
  252.9 0.1 fusion.71
  253.1 2.4 fusion.35
  255.5 0.3 concatenate.73
  255.8 3.4 %collective-permute-start = (bf16[128,128]{1,0:T(8,128)(2,1)S(1)}, bf16[128,128]{1,0:T(8,128)(2,1)S(1)}, u32[]{:S(2)}, u32[]{:S(2)}) collective-permute-start(bf16[128,128]{1,0:T(8,128)(2,1)S(1)} %get-tuple-element.24), channel_id=1, source_target_pairs={{0,4},{4,8},{8,12},{12,16},{16,20},{20,24},{24,28},{1,5},{5,9},{9,... | collective-permute-start | bytes 98312 | tf_op jit(solution)/shard_map/ppermute | solution.py:18
  259.1 1.3 collective-permute-start.1
  260.4 1.3 collective-permute-start.3
  261.7 5.2 %collective-permute-start.2 = (bf16[1,256]{1,0:T(2,128)(2,1)S(1)}, bf16[1,256]{1,0:T(2,128)(2,1)S(1)}, u32[]{:S(2)}, u32[]{:S(2)}) collective-permute-start(bf16[1,256]{1,0:T(2,128)(2,1)S(1)} %get-tuple-element.16), channel_id=1, source_target_pairs={{0,4},{4,8},{8,12},{12,16},{16,20},{20,24},{24,28},{1,5},{5,9},{9,... | collective-permute-start | bytes 1544 | tf_op jit(solution)/shard_map/ppermute | solution.py:18
  266.9 0.1 copy.54
  267.0 0.1 copy.53
  267.1 0.1 copy.52
  267.2 0.1 copy.51
  267.3 0.1 copy.49
  267.4 0.8 collective-permute-done.2
  268.2 0.1 maximum_convert_fusion
  268.3 0.1 fusion.70
  268.4 0.1 copy.56
  268.6 0.1 copy.55
  268.7 0.1 copy.50
  268.8 0.1 copy.48
  268.9 0.6 fusion.4
  269.6 0.1 broadcast_maximum_fusion
  269.6 0.7 fusion.3
  270.3 0.1 exponential_add_fusion
  270.4 1.0 fusion.14
  271.3 0.2 copy.63
  271.6 13.1 %all-gather.19.cloned.1.call-done = bf16[256,2048]{1,0:T(8,128)(2,1)} async-done(((bf16[256,256]{1,0:T(8,128)(2,1)}), bf16[256,2048]{1,0:T(8,128)(2,1)}) %all-gather.19.cloned.1.call-update) | async-done | bytes 1048592 | tf_op jit(solution)/shard_map/all_gather | solution.py:176
  284.7 2.0 fusion.41
  286.6 3.2 add_convert_fusion
  289.8 0.7 fusion.77
  290.5 29.6 %reduce-scatter.2.cloned.1.call-done = bf16[128,2048]{1,0:T(8,128)(2,1)} async-done(((bf16[512,2048]{1,0:T(8,128)(2,1)}), bf16[128,2048]{1,0:T(8,128)(2,1)}) %reduce-scatter.2.cloned.1.call-update) | async-done | bytes 524304 | tf_op jit(solution)/shard_map/reduce_scatter | solution.py:179
  (25 shorter events, 0.3 us)
Async XLA Ops:
  7.2 74.9 %all-gather.21.cloned.1.call-start = ((), (), s32[]{:S(2)}) async-start(), calls=%async_computation.8 | async-start | bytes 1179648 | tf_op jit(solution)/shard_map/all_gather | solution.py:177
  7.9 89.4 %all-gather.11.cloned.1.call-start = ((), (), s32[]{:S(2)}) async-start(), calls=%async_computation.2 | async-start | bytes 1179648 | tf_op jit(solution)/shard_map/all_gather | solution.py:89
  8.6 129.8 %all-gather.13.cloned.1.call-start = ((), (), s32[]{:S(2)}) async-start(), calls=%async_computation.3 | async-start | bytes 1179648 | tf_op jit(solution)/shard_map/all_gather | solution.py:92
  9.4 170.0 %all-gather.15.cloned.1.call-start = ((), (), s32[]{:S(2)}) async-start(), calls=%async_computation.4 | async-start | bytes 1179648 | tf_op jit(solution)/shard_map/all_gather | solution.py:93
  10.0 210.5 %all-gather.17.cloned.1.call-start = ((), (), s32[]{:S(2)}) async-start(), calls=%async_computation.5 | async-start | bytes 1179648 | tf_op jit(solution)/shard_map/all_gather | solution.py:94
  10.5 232.6 %all-gather.9.cloned.1.call-start = ((), (), s32[]{:S(2)}) async-start(), calls=%async_computation.1 | async-start | bytes 2621440 | tf_op jit(solution)/shard_map/all_gather | solution.py:74
  11.1 273.5 %all-gather.19.cloned.1.call-start = ((), (), s32[]{:S(2)}) async-start(), calls=%async_computation.6 | async-start | bytes 1179648 | tf_op jit(solution)/shard_map/all_gather | solution.py:176
  11.9 308.2 %reduce-scatter.2.cloned.1.call-start = ((), (), s32[]{:S(2)}) async-start(), calls=%async_computation.7 | async-start | bytes 2621440 | tf_op jit(solution)/shard_map/reduce_scatter | solution.py:179
  83.5 161.7 %copy-start.2 = (f32[2048]{0:T(1024)S(1)}, f32[2048]{0:T(1024)}, u32[]{:S(2)}) copy-start(f32[2048]{0:T(1024)} %param.13) | copy-start | bytes 24580
  251.2 1.4 copy-start
  255.8 12.5 %collective-permute-start = (bf16[128,128]{1,0:T(8,128)(2,1)S(1)}, bf16[128,128]{1,0:T(8,128)(2,1)S(1)}, u32[]{:S(2)}, u32[]{:S(2)}) collective-permute-start(bf16[128,128]{1,0:T(8,128)(2,1)S(1)} %get-tuple-element.24), channel_id=1, source_target_pairs={{0,4},{4,8},{8,12},{12,16},{16,20},{20,24},{24,28},{1,5},{5,9},{9,... | collective-permute-start | bytes 98312 | tf_op jit(solution)/shard_map/ppermute | solution.py:18
  259.1 9.2 %collective-permute-start.1 = (bf16[128,128]{1,0:T(8,128)(2,1)S(1)}, bf16[128,128]{1,0:T(8,128)(2,1)S(1)}, u32[]{:S(2)}, u32[]{:S(2)}) collective-permute-start(bf16[128,128]{1,0:T(8,128)(2,1)S(1)} %get-tuple-element.25), channel_id=1, source_target_pairs={{4,0},{8,4},{12,8},{16,12},{20,16},{24,20},{28,24},{5,1},{9,5},{13... | collective-permute-start | bytes 98312 | tf_op jit(solution)/shard_map/ppermute | solution.py:21
  260.4 7.0 %collective-permute-start.3 = (bf16[1,256]{1,0:T(2,128)(2,1)S(1)}, bf16[1,256]{1,0:T(2,128)(2,1)S(1)}, u32[]{:S(2)}, u32[]{:S(2)}) collective-permute-start(bf16[1,256]{1,0:T(2,128)(2,1)S(1)} %get-tuple-element.17), channel_id=1, source_target_pairs={{4,0},{8,4},{12,8},{16,12},{20,16},{24,20},{28,24},{5,1},{9,5},{13... | collective-permute-start | bytes 1544 | tf_op jit(solution)/shard_map/ppermute | solution.py:21
  261.7 6.5 %collective-permute-start.2 = (bf16[1,256]{1,0:T(2,128)(2,1)S(1)}, bf16[1,256]{1,0:T(2,128)(2,1)S(1)}, u32[]{:S(2)}, u32[]{:S(2)}) collective-permute-start(bf16[1,256]{1,0:T(2,128)(2,1)S(1)} %get-tuple-element.16), channel_id=1, source_target_pairs={{0,4},{4,8},{8,12},{12,16},{16,20},{20,24},{24,28},{1,5},{5,9},{9,... | collective-permute-start | bytes 1544 | tf_op jit(solution)/shard_map/ppermute | solution.py:18
  268.4 1.1 copy-start.1
Sparse Core Ops, SparseCore 0:
  10.1 45.7 all-gather.20
  58.0 39.2 all-gather.10
  99.5 38.9 all-gather.12
  140.4 38.9 all-gather.14
  181.4 38.9 all-gather.16
  221.8 21.2 all-gather.8
  245.2 39.4 all-gather.18
  289.9 30.0 reduce-scatter.1
